TPU v7x, 32 devices: a whole 2x2x4 slice. The times are simulated.
32 devices in a mesh: sp: 16 (over z, y, core), tp: 2 (over x).
Axes of the slice: x: 2, y: 2, z: 4, core: 2. Of those that a mesh axis runs over, the one named last changes fastest.
Arguments:
- residual: bfloat16 [2048, 2048], P(('sp', 'tp')), may hold values from -6 to 6
- q_small: bfloat16 [2048, 1024], P('sp', 'tp'), may hold values from -6 to 6
- k_small: bfloat16 [2048, 1024], P('sp', 'tp'), may hold values from -6 to 6
- v_small: bfloat16 [2048, 1024], P('sp', 'tp'), may hold values from -6 to 6
- q_large: bfloat16 [2048, 1024], P('sp', 'tp'), may hold values from -6 to 6
- k_large: bfloat16 [2048, 1024], P('sp', 'tp'), may hold values from -6 to 6
- v_large: bfloat16 [2048, 1024], P('sp', 'tp'), may hold values from -6 to 6
- forget_small: float32 [2048, 16], P('sp', 'tp'), may hold values from 0 to 20
- forget_large: float32 [2048, 8], P('sp', 'tp'), may hold values from 0 to 20
- w_out_small: bfloat16 [1024, 2048], P('tp'), may hold values from -0.125 to 0.125
- w_out_large: bfloat16 [1024, 2048], P('tp'), may hold values from -0.125 to 0.125
- norm_gain: float32 [2048], replicated, may hold values from 0.1 to 1.9
- w_gate: bfloat16 [2048, 4096], P('sp', 'tp'), may hold values from -0.125 to 0.125
- w_up: bfloat16 [2048, 4096], P('sp', 'tp'), may hold values from -0.125 to 0.125
- conv_gate: float32 [3, 4096], P(None, 'tp'), may hold values from -3 to 3
- conv_up: float32 [3, 4096], P(None, 'tp'), may hold values from -3 to 3
- w_down: bfloat16 [4096, 2048], P('tp', 'sp'), may hold values from -0.09375 to 0.09375
Outputs:
- mixed: bfloat16 [2048, 2048], P(('sp', 'tp'))
All inputs are finite; a program needn't handle non-finite values.
Results may differ from a plain program's by a relative error of at most 0.015.
Values may be sent and summed in bfloat16 or wider, within the bound.
A program may use at most 64 MiB of HBM per device.

v0:
```python
import jax
import jax.numpy as jnp
from jax import lax
from jax.sharding import PartitionSpec as P

EPS = 1e-06
NEG = -1e30


def from_behind(block, axis, distance):
    devices = range(lax.axis_size(axis))
    route = [(i - distance, i) for i in devices if i - distance in devices]
    return lax.ppermute(block, axis, route)


def globalize(part, rows):
    heads = part.shape[1]
    blocks = part.reshape(-1, rows, heads)
    totals = blocks[:, -1, :]
    before = jnp.cumsum(totals, axis=0) - totals
    return (blocks + before[:, None, :]).reshape(part.shape)


def attend(carry, keys, values, queries, cum_own, cum_every, qpos):
    top, denom, accum = carry
    count = keys.shape[0]
    heads = queries.shape[1]
    size = queries.shape[2]
    keys = keys.reshape(count, heads, size)
    values = values.reshape(count, heads, size)
    kpos = jnp.arange(count, dtype=jnp.int32)
    scores = jnp.einsum(
        "qhd,khd->qhk", queries, keys, preferred_element_type=jnp.float32
    ) * size ** (-0.5)
    scores = scores + cum_own[:, :, None] - cum_every.T[None, :, :]
    keep = (kpos[None, :] <= qpos[:, None])[:, None, :]
    scores = jnp.where(keep, scores, NEG)
    new_top = jnp.maximum(top, jnp.max(scores, axis=-1))
    weights = jnp.where(keep, jnp.exp(scores - new_top[:, :, None]), 0.0)
    denom = jnp.sum(weights, axis=-1)
    accum = jnp.einsum(
        "qhk,khd->qhd", weights.astype(jnp.bfloat16), values, preferred_element_type=jnp.float32
    )
    return (new_top, denom, accum)


def finish(carry):
    top, denom, accum = carry
    attended = accum / denom[:, :, None]
    normed = attended * lax.rsqrt(jnp.mean(attended * attended, axis=-1, keepdims=True) + EPS)
    return normed.astype(jnp.bfloat16).reshape(attended.shape[0], -1)


def empty_carry(rows, heads, size):
    return (
        jnp.full((rows, heads), NEG, jnp.float32),
        jnp.zeros((rows, heads), jnp.float32),
        jnp.zeros((rows, heads, size), jnp.float32),
    )


def body(
    residual,
    q_small,
    k_small,
    v_small,
    q_large,
    k_large,
    v_large,
    forget_small,
    forget_large,
    w_out_small,
    w_out_large,
    norm_gain,
    w_gate,
    w_up,
    conv_gate,
    conv_up,
    w_down,
):
    rows = q_small.shape[0]
    offset = lax.axis_index("sp") * rows
    qpos = offset + jnp.arange(rows, dtype=jnp.int32)
    gathered = (
        lax.all_gather(w_gate, "sp", axis=0, tiled=True),
        lax.all_gather(w_up, "sp", axis=0, tiled=True),
        lax.all_gather(w_down, "sp", axis=1, tiled=True),
    )
    local_small = jnp.cumsum(jax.nn.log_sigmoid(forget_small), axis=0)
    local_large = jnp.cumsum(jax.nn.log_sigmoid(forget_large), axis=0)
    part_small, part_large = (
        lax.all_gather(local_small, "sp", axis=0, tiled=True),
        lax.all_gather(local_large, "sp", axis=0, tiled=True),
    )
    every_small = globalize(part_small, rows)
    every_large = globalize(part_large, rows)
    cum_small = lax.dynamic_slice_in_dim(every_small, offset, rows, 0)
    cum_large = lax.dynamic_slice_in_dim(every_large, offset, rows, 0)
    heads_small = forget_small.shape[1]
    heads_large = forget_large.shape[1]
    queries_small = q_small.reshape(rows, heads_small, -1)
    queries_large = q_large.reshape(rows, heads_large, -1)
    start_carry = (
        empty_carry(rows, heads_small, queries_small.shape[2]),
        empty_carry(rows, heads_large, queries_large.shape[2]),
    )
    keys_s = lax.all_gather(k_small, "sp", axis=0, tiled=True)
    values_s = lax.all_gather(v_small, "sp", axis=0, tiled=True)
    keys_l = lax.all_gather(k_large, "sp", axis=0, tiled=True)
    values_l = lax.all_gather(v_large, "sp", axis=0, tiled=True)
    small = attend(start_carry[0], keys_s, values_s, queries_small, cum_small, every_small, qpos)
    large = attend(start_carry[1], keys_l, values_l, queries_large, cum_large, every_large, qpos)
    normed_small = finish(small)
    normed_large = finish(large)
    first_part = jnp.dot(normed_small, w_out_small, preferred_element_type=jnp.float32)
    projected = lax.psum_scatter(
        (
            first_part + jnp.dot(normed_large, w_out_large, preferred_element_type=jnp.float32)
        ).astype(jnp.bfloat16),
        "tp",
        scatter_dimension=0,
        tiled=True,
    ).astype(jnp.float32)
    first = residual.astype(jnp.float32) + projected
    normal = (
        first * lax.rsqrt(jnp.mean(first * first, axis=-1, keepdims=True) + EPS) * norm_gain
    ).astype(jnp.bfloat16)
    gate_full, up_full, down_full = gathered
    piece = lax.all_gather(normal, "tp", axis=0, tiled=True)
    gate_part = jnp.dot(piece, gate_full, preferred_element_type=jnp.float32).astype(jnp.bfloat16)
    up_part = jnp.dot(piece, up_full, preferred_element_type=jnp.float32).astype(jnp.bfloat16)
    both = jnp.concatenate([gate_part, up_part], axis=1)
    width = both.shape[0]
    rim = from_behind(both[width - 2 :], "sp", 1)
    extended = jnp.concatenate([rim, both], axis=0).astype(jnp.float32)
    taps = jnp.concatenate([conv_gate, conv_up], axis=1)
    conv = (
        taps[0] * extended[0:width]
        + taps[1] * extended[1 : width + 1]
        + taps[2] * extended[2 : width + 2]
    )
    half = gate_full.shape[1]
    hidden = (jax.nn.silu(conv[:, :half]) * conv[:, half:]).astype(jnp.bfloat16)
    mixed = first + lax.psum_scatter(
        jnp.dot(hidden, down_full, preferred_element_type=jnp.float32).astype(jnp.bfloat16),
        "tp",
        scatter_dimension=0,
        tiled=True,
    ).astype(jnp.float32)
    return mixed.astype(jnp.bfloat16)


def solution(mesh):
    placed = (
        P(("sp", "tp"), None),
        P("sp", "tp"),
        P("sp", "tp"),
        P("sp", "tp"),
        P("sp", "tp"),
        P("sp", "tp"),
        P("sp", "tp"),
        P("sp", "tp"),
        P("sp", "tp"),
        P("tp", None),
        P("tp", None),
        P(),
        P("sp", "tp"),
        P("sp", "tp"),
        P(None, "tp"),
        P(None, "tp"),
        P("tp", "sp"),
    )
    return jax.shard_map(
        body, mesh=mesh, in_specs=placed, out_specs=P(("sp", "tp"), None), check_vma=False
    )
```

profile of v0, /device:TPU:0, one launch (start us, length us, event | category | flops | bytes accessed | tf_op | source)
XLA Modules:
  0.0 472.0 jit_solution(16428870450614130786)
XLA Ops:
  6.5 0.7 all-gather.14.cloned.1.call-update
  7.3 0.0 all-gather.8.cloned.1.call-start
  7.3 0.7 all-gather.8.cloned.1.call-update
  8.0 0.0 all-gather.12.cloned.1.call-start
  8.1 1.7 copy.44
  9.7 0.0 all-gather.10.cloned.1.call-start
  9.8 0.5 all-gather.10.cloned.1.call-update
  10.3 0.0 reduce-scatter.3.cloned.1.call-start
  10.4 0.7 fusion.40
  11.1 0.1 copy.47
  11.2 0.2 reduce_window_sum.46
  11.4 27.1 %all_gather.34 = f32[2048,4]{1,0:T(8,128)S(1)} all-gather(f32[128,4]{1,0:T(8,128)S(1)} %reduce_window_sum.46), channel_id=1, replica_groups=mesh['sp'=16,'tp'=2] {'sp'}, dimensions={0}, use_global_device_ids=true | all-gather | bytes 34816 | tf_op jit(solution)/shard_map/all_gather | solution.py:93
  38.5 0.1 bitcast_add_fusion.2
  38.6 0.1 copy.37
  38.7 0.2 reduce_window_sum.44
  38.8 24.5 %all_gather.31 = f32[2048,8]{1,0:T(8,128)S(1)} all-gather(f32[128,8]{1,0:T(8,128)S(1)} %reduce_window_sum.44), channel_id=1, replica_groups=mesh['sp'=16,'tp'=2] {'sp'}, dimensions={0}, use_global_device_ids=true | all-gather | bytes 69632 | tf_op jit(solution)/shard_map/all_gather | solution.py:92
  63.4 1.1 bitcast_add_fusion.3
  64.4 0.8 constant_dynamic-slice_fusion.1
  65.3 0.1 copy.50
  65.4 0.3 copy.51
  65.7 0.1 copy.40
  65.7 1.6 copy.41
  67.3 0.1 copy.36
  67.4 0.2 iota_compare_fusion
  67.7 4.0 copy.52
  71.7 31.4 %all-gather.8.cloned.1.call-done = bf16[2048,512]{1,0:T(8,128)(2,1)} async-done(((bf16[128,512]{1,0:T(8,128)(2,1)}), bf16[2048,512]{1,0:T(8,128)(2,1)}) %all-gather.8.cloned.1.call-update) | async-done | bytes 2097168 | tf_op jit(solution)/shard_map/all_gather | solution.py:107
  103.0 4.0 copy.35
  107.0 38.0 %all-gather.12.cloned.1.call-done = bf16[2048,512]{0,1:T(8,128)(2,1)} async-done(((bf16[128,512]{0,1:T(8,128)(2,1)}), bf16[2048,512]{0,1:T(8,128)(2,1)}) %all-gather.12.cloned.1.call-update) | async-done | bytes 2097168 | tf_op jit(solution)/shard_map/all_gather | solution.py:109
  145.0 3.7 fusion.47
  148.7 0.8 fusion.10
  149.5 0.8 copy-done.7
  150.3 1.2 multiply_reduce_fusion.1
  151.4 0.4 copy-done.6
  151.9 3.4 fusion.4
  155.3 3.2 copy-done.2
  158.5 3.1 fusion.2
  161.6 26.0 %all-gather.10.cloned.1.call-done = bf16[2048,512]{1,0:T(8,128)(2,1)} async-done(((bf16[128,512]{1,0:T(8,128)(2,1)}), bf16[2048,512]{1,0:T(8,128)(2,1)}) %all-gather.10.cloned.1.call-update) | async-done | bytes 2097168 | tf_op jit(solution)/shard_map/all_gather | solution.py:108
  187.6 3.9 copy.42
  191.5 6.6 %multiply_reduce_fusion.2 = (f32[128,8]{0,1:T(8,128)S(1)}, f32[128,8,64]{0,2,1:T(8,128)S(1)}) fusion(f32[128,8]{0,1:T(8,128)S(1)} %fusion.2, bf16[2048,8,64]{0,2,1:T(8,128)(2,1)} %bitcast.82, f32[8,2048,128]{2,1,0:T(8,128)} %copy-done.2, f32[128,8]{0,1:T(8,128)S(1)} %broadcast_maximum_fusion, f32[8,2048]{1,0:T(8,128)S(1)} %copy.41, f32[128,8]{0,1:T(8,128)S(1)} %copy.40, ...), kind=kOutput, calls=%fused_computation.49 | convolution fusion | flops 283311104 | bytes 11091968 | tf_op jit(solution)/shard_map/qhk,khd->qhd/dot_general | solution.py:41
  198.3 0.5 fusion.48
  198.8 1.0 copy-done.5
  199.7 1.3 fusion.12
  201.1 0.0 all-gather.18.cloned.1.call-start
  201.1 0.5 all-gather.18.cloned.1.call-update
  201.6 0.0 all-gather.16.cloned.1.call-start
  201.7 0.7 all-gather.16.cloned.1.call-update
  202.4 0.7 all-gather.20.cloned.1.call-update
  203.1 0.0 reduce-scatter.5.cloned.1.call-start
  203.2 11.3 %reduce-scatter.3.cloned.1.call-done = bf16[64,2048]{1,0:T(8,128)(2,1)} async-done(((bf16[128,2048]{1,0:T(8,128)(2,1)}), bf16[64,2048]{1,0:T(8,128)(2,1)}) %reduce-scatter.3.cloned.1.call-update) | async-done | bytes 262160 | tf_op jit(solution)/shard_map/reduce_scatter | solution.py:116
  214.6 1.1 multiply_reduce_fusion
  215.7 1.1 multiply_convert_fusion
  216.8 8.7 %all_gather.36 = bf16[128,2048]{1,0:T(8,128)(2,1)S(1)} all-gather(bf16[64,2048]{1,0:T(8,128)(2,1)S(1)} %multiply_convert_fusion), channel_id=1, replica_groups=mesh['sp'=16,'tp'=2] {'tp'}, dimensions={0}, use_global_device_ids=true | all-gather | bytes 786432 | tf_op jit(solution)/shard_map/all_gather | solution.py:129
  225.5 65.4 %all-gather.18.cloned.1.call-done = bf16[2048,2048]{1,0:T(8,128)(2,1)} async-done(((bf16[128,2048]{1,0:T(8,128)(2,1)}), bf16[2048,2048]{1,0:T(8,128)(2,1)}) %all-gather.18.cloned.1.call-update) | async-done | bytes 8388624 | tf_op jit(solution)/shard_map/all_gather | solution.py:86
  290.9 4.6 convolution_convert_fusion.1
  295.6 70.4 %all-gather.16.cloned.1.call-done = bf16[2048,2048]{1,0:T(8,128)(2,1)} async-done(((bf16[128,2048]{1,0:T(8,128)(2,1)}), bf16[2048,2048]{1,0:T(8,128)(2,1)}) %all-gather.16.cloned.1.call-update) | async-done | bytes 8388624 | tf_op jit(solution)/shard_map/all_gather | solution.py:85
  366.0 4.6 convolution_convert_fusion.2
  370.7 2.2 collective-permute-start
  372.9 0.8 collective-permute-done
  373.6 0.3 maximum_convert_fusion
  373.9 2.0 fusion.15
  375.9 68.5 %all-gather.20.cloned.1.call-done = bf16[2048,2048]{1,0:T(8,128)(2,1)} async-done(((bf16[2048,128]{1,0:T(8,128)(2,1)}), bf16[2048,2048]{1,0:T(8,128)(2,1)}) %all-gather.20.cloned.1.call-update) | async-done | bytes 8388624 | tf_op jit(solution)/shard_map/all_gather | solution.py:87
  444.5 6.3 %convolution_convert_fusion = bf16[128,2048]{1,0:T(8,128)(2,1)} fusion(bf16[2048,2048]{1,0:T(8,128)(2,1)} %all-gather.20.cloned.1.call-done, f32[128,4096]{1,0:T(8,128)} %fusion.15), kind=kOutput, calls=%fused_computation.16 | convolution fusion | flops 1075576832 | bytes 11010048 | tf_op jit(solution)/shard_map/dot_general | solution.py:145
  450.8 13.0 %reduce-scatter.5.cloned.1.call-done = bf16[64,2048]{1,0:T(8,128)(2,1)} async-done(((bf16[128,2048]{1,0:T(8,128)(2,1)}), bf16[64,2048]{1,0:T(8,128)(2,1)}) %reduce-scatter.5.cloned.1.call-update) | async-done | bytes 262160 | tf_op jit(solution)/shard_map/reduce_scatter | solution.py:144
  463.8 1.7 add_convert_fusion
  (46 shorter events, 0.4 us)
Async XLA Ops:
  6.5 191.7 %copy-start = (bf16[512,2048]{1,0:T(8,128)(2,1)S(1)}, bf16[512,2048]{1,0:T(8,128)(2,1)}, u32[]{:S(2)}) copy-start(bf16[512,2048]{1,0:T(8,128)(2,1)} %param.26) | copy-start | bytes 6291460
  6.5 32.0 %copy-start.12 = (f32[128,8]{0,1:T(8,128)S(1)}, f32[128,8]{0,1:T(8,128)}, u32[]{:S(2)}) copy-start(f32[128,8]{0,1:T(8,128)} %param.24) | copy-start | bytes 12292
  6.5 61.1 %all-gather.14.cloned.1.call-start = ((), (), s32[]{:S(2)}) async-start(), calls=%async_computation.5 | async-start | bytes 2228224 | tf_op jit(solution)/shard_map/all_gather | solution.py:110
  7.3 95.8 %all-gather.8.cloned.1.call-start = ((), (), s32[]{:S(2)}) async-start(), calls=%async_computation.2 | async-start | bytes 2228224 | tf_op jit(solution)/shard_map/all_gather | solution.py:107
  8.0 137.0 %all-gather.12.cloned.1.call-start = ((), (), s32[]{:S(2)}) async-start(), calls=%async_computation.4 | async-start | bytes 2228224 | tf_op jit(solution)/shard_map/all_gather | solution.py:109
  9.7 177.8 %all-gather.10.cloned.1.call-start = ((), (), s32[]{:S(2)}) async-start(), calls=%async_computation.3 | async-start | bytes 2228224 | tf_op jit(solution)/shard_map/all_gather | solution.py:108
  10.3 204.2 %reduce-scatter.3.cloned.1.call-start = ((), (), s32[]{:S(2)}) async-start(), calls=%async_computation.6 | async-start | bytes 786432 | tf_op jit(solution)/shard_map/reduce_scatter | solution.py:116
  38.4 28.9 %copy-start.8 = (bf16[128,512]{1,0:T(8,128)(2,1)S(1)}, bf16[128,512]{1,0:T(8,128)(2,1)}, u32[]{:S(2)}) copy-start(bf16[128,512]{1,0:T(8,128)(2,1)} %param.18) | copy-start | bytes 393220
  67.6 77.4 %copy-start.13 = (bf16[128,512]{1,0:T(8,128)(2,1)S(1)}, bf16[128,512]{1,0:T(8,128)(2,1)}, u32[]{:S(2)}) copy-start(bf16[128,512]{1,0:T(8,128)(2,1)} %param.21) | copy-start | bytes 393220
  148.7 1.6 copy-start.7
  150.3 1.6 copy-start.6
  155.2 3.2 copy-start.2
  198.1 1.6 copy-start.5
  198.2 5.0 %copy-start.9 = (f32[3,2048]{1,0:T(4,128)S(1)}, f32[3,2048]{1,0:T(4,128)}, u32[]{:S(2)}) copy-start(f32[3,2048]{1,0:T(4,128)} %param.31) | copy-start | bytes 73732
  198.2 5.0 %copy-start.10 = (f32[3,2048]{1,0:T(4,128)S(1)}, f32[3,2048]{1,0:T(4,128)}, u32[]{:S(2)}) copy-start(f32[3,2048]{1,0:T(4,128)} %param.32) | copy-start | bytes 73732
  198.3 16.3 %copy-start.3 = (bf16[64,2048]{1,0:T(8,128)(2,1)S(1)}, bf16[64,2048]{1,0:T(8,128)(2,1)}, u32[]{:S(2)}) copy-start(bf16[64,2048]{1,0:T(8,128)(2,1)} %param.17) | copy-start | bytes 786436
  198.3 17.5 %copy-start.11 = (f32[2048]{0:T(1024)S(1)}, f32[2048]{0:T(1024)}, u32[]{:S(2)}) copy-start(f32[2048]{0:T(1024)} %param.28) | copy-start | bytes 24580
  201.1 89.8 %all-gather.18.cloned.1.call-start = ((), (), s32[]{:S(2)}) async-start(), calls=%async_computation.8 | async-start | bytes 8912896 | tf_op jit(solution)/shard_map/all_gather | solution.py:86
  201.6 164.3 %all-gather.16.cloned.1.call-start = ((), (), s32[]{:S(2)}) async-start(), calls=%async_computation.7 | async-start | bytes 8912896 | tf_op jit(solution)/shard_map/all_gather | solution.py:85
  202.4 242.1 %all-gather.20.cloned.1.call-start = ((), (), s32[]{:S(2)}) async-start(), calls=%async_computation.9 | async-start | bytes 8912896 | tf_op jit(solution)/shard_map/all_gather | solution.py:87
  203.1 260.6 %reduce-scatter.5.cloned.1.call-start = ((), (), s32[]{:S(2)}) async-start(), calls=%async_computation.10 | async-start | bytes 786432 | tf_op jit(solution)/shard_map/reduce_scatter | solution.py:144
  370.7 3.0 collective-permute-start
  375.9 87.8 %copy-start.4 = (bf16[64,2048]{1,0:T(8,128)(2,1)S(1)}, bf16[64,2048]{1,0:T(8,128)(2,1)}, u32[]{:S(2)}) copy-start(bf16[64,2048]{1,0:T(8,128)(2,1)} %reduce-scatter.3.cloned.1.call-done) | copy-start | bytes 786436
  444.5 21.0 %copy-start.1 = (bf16[512,2048]{1,0:T(8,128)(2,1)S(1)}, bf16[512,2048]{1,0:T(8,128)(2,1)}, u32[]{:S(2)}) copy-start(bf16[512,2048]{1,0:T(8,128)(2,1)} %param.26) | copy-start | bytes 6291460
Sparse Core Ops, SparseCore 0:
  9.5 49.7 all-gather.13
  61.4 41.5 all-gather.7
  105.2 39.7 all-gather.11
  147.0 40.5 all-gather.9
  201.2 13.3 reduce-scatter.2
  216.6 74.2 all-gather.17
  293.1 72.8 all-gather.15
  368.1 76.2 all-gather.19
  450.9 12.7 reduce-scatter.4
where the time goes:
time: 473 us; the launch traced here: 472 us
  waiting for transfers between devices  329 us (70%)
  blocking collectives  60.3 us (13%)
  matrix products  32.2 us (7%)
  local copies, waits for them, and re-layouts  22.4 us (5%)
  between operations  13.5 us (3%)
  other arithmetic  12.6 us (3%)
    all_gather x1, waiting for transfers between devices, body(): lax.all_gather(w_gate, 'sp', axis=0, tiled=True)  70.4 us
    all_gather x1, waiting for transfers between devices, body(): lax.all_gather(w_down, 'sp', axis=1, tiled=True)  68.5 us
    all_gather x1, waiting for transfers between devices, body(): lax.all_gather(w_up, 'sp', axis=0, tiled=True)  65.4 us
    all_gather x1, waiting for transfers between devices, body(): keys_l = lax.all_gather(k_large, 'sp', axis=0, tiled=True)  38 us
    all_gather x1, waiting for transfers between devices, body(): keys_s = lax.all_gather(k_small, 'sp', axis=0, tiled=True)  31.4 us
    all_gather x1, blocking collectives, body(): lax.all_gather(local_large, 'sp', axis=0, tiled=True)  27.1 us
    all_gather x1, waiting for transfers between devices, body(): values_s = lax.all_gather(v_small, 'sp', axis=0, tiled=True)  26 us
    all_gather x1, blocking collectives, body(): lax.all_gather(local_small, 'sp', axis=0, tiled=True)  24.5 us
  transfers between devices with their start and end apart: 10, of which 9 were waited for; matrix products, arithmetic and copies ran while one was open for 9% of the time, Pallas kernels for 0%

commit v1 on v0

--- a/solution.py
+++ b/solution.py
@@ -105,8 +105,11 @@
         empty_carry(rows, heads_large, queries_large.shape[2]),
     )
     keys_s = lax.all_gather(k_small, "sp", axis=0, tiled=True)
-    values_s = lax.all_gather(v_small, "sp", axis=0, tiled=True)
-    keys_l = lax.all_gather(k_large, "sp", axis=0, tiled=True)
+    values_s, keys_l = jnp.split(
+        lax.all_gather(jnp.concatenate([v_small, k_large], axis=1), "sp", axis=0, tiled=True),
+        [v_small.shape[1]],
+        axis=1,
+    )
     values_l = lax.all_gather(v_large, "sp", axis=0, tiled=True)
     small = attend(start_carry[0], keys_s, values_s, queries_small, cum_small, every_small, qpos)
     large = attend(start_carry[1], keys_l, values_l, queries_large, cum_large, every_large, qpos)

time: 473 us -> 441 us (0.932)
  waiting for transfers between devices: 329 us -> 303 us
    all_gather x2 -> x1, waiting for transfers between devices: 64 us -> 36.6 us  [body(): lax.all_gather(jnp.concatenate([v_small, k_large], axis=1), 'sp', axis=0,...]
  transfers between devices with their start and end apart: 10 -> 9, of which waited for: 9 -> 8; matrix products, arithmetic and copies ran while one was open for 9% -> 8% of each run, Pallas kernels for 0% -> 0%
where the time goes in v1:
time: 441 us; the launch traced here: 440 us
  waiting for transfers between devices  303 us (69%)
  blocking collectives  59.2 us (13%)
  matrix products  30.1 us (7%)
  local copies, waits for them, and re-layouts  18.9 us (4%)
  between operations  13.9 us (3%)
  other arithmetic  12.3 us (3%)
    all_gather x1, waiting for transfers between devices, body(): lax.all_gather(w_gate, 'sp', axis=0, tiled=True)  70.3 us
    all_gather x1, waiting for transfers between devices, body(): lax.all_gather(w_down, 'sp', axis=1, tiled=True)  68.5 us
    all_gather x1, waiting for transfers between devices, body(): lax.all_gather(w_up, 'sp', axis=0, tiled=True)  65.6 us
    all_gather x1, waiting for transfers between devices, body(): lax.all_gather(jnp.concatenate([v_small, k_large], axis=1), 'sp', axis=0,...  36.6 us
    all_gather x1, waiting for transfers between devices, body(): keys_s = lax.all_gather(k_small, 'sp', axis=0, tiled=True)  34.2 us
    all_gather x1, blocking collectives, body(): lax.all_gather(local_large, 'sp', axis=0, tiled=True)  26.9 us
    all_gather x1, blocking collectives, body(): lax.all_gather(local_small, 'sp', axis=0, tiled=True)  23.8 us
    reduce_scatter x1, waiting for transfers between devices, body(): lax.psum_scatter(jnp.dot(hidden, down_full, preferred_element_type=jnp.fl...  13 us
  transfers between devices with their start and end apart: 9, of which 8 were waited for; matrix products, arithmetic and copies ran while one was open for 8% of the time, Pallas kernels for 0%

profile of v1, /device:TPU:0, one launch (start us, length us, event | category | flops | bytes accessed | tf_op | source)
XLA Modules:
  0.0 439.9 jit_solution(10688019138226025006)
XLA Ops:
  6.5 0.7 all-gather.11.cloned.1.call-update
  7.3 0.0 all-gather.9.cloned.1.call-start
  7.3 0.7 all-gather.9.cloned.1.call-update
  8.0 0.0 all-gather.7.cloned.1.call-start
  8.1 1.0 copy.35
  9.1 1.0 copy.36
  10.1 0.7 pad_maximum_fusion
  10.8 0.0 all-gather.7.cloned.1.call-update
  10.9 0.0 reduce-scatter.3.cloned.1.call-start
  10.9 0.7 fusion.40
  11.6 0.1 copy.47
  11.7 0.2 reduce_window_sum.46
  11.9 26.9 %all_gather.30 = f32[2048,4]{1,0:T(8,128)S(1)} all-gather(f32[128,4]{1,0:T(8,128)S(1)} %reduce_window_sum.46), channel_id=1, replica_groups=mesh['sp'=16,'tp'=2] {'sp'}, dimensions={0}, use_global_device_ids=true | all-gather | bytes 34816 | tf_op jit(solution)/shard_map/all_gather | solution.py:93
  38.8 0.1 bitcast_add_fusion.2
  38.9 0.1 copy.50
  39.0 0.3 copy.51
  39.3 0.1 copy.39
  39.4 0.2 reduce_window_sum.44
  39.6 23.8 %all_gather.29 = f32[2048,8]{1,0:T(8,128)S(1)} all-gather(f32[128,8]{1,0:T(8,128)S(1)} %reduce_window_sum.44), channel_id=1, replica_groups=mesh['sp'=16,'tp'=2] {'sp'}, dimensions={0}, use_global_device_ids=true | all-gather | bytes 69632 | tf_op jit(solution)/shard_map/all_gather | solution.py:92
  63.4 0.1 bitcast_add_fusion.3
  63.6 0.3 copy.43
  63.9 0.1 copy.38
  64.0 0.2 iota_compare_fusion
  64.2 0.0 all-gather.11.cloned.1.call-done
  64.2 4.0 copy.52
  68.2 34.2 %all-gather.9.cloned.1.call-done = bf16[2048,512]{1,0:T(8,128)(2,1)} async-done(((bf16[128,512]{1,0:T(8,128)(2,1)}), bf16[2048,512]{1,0:T(8,128)(2,1)}) %all-gather.9.cloned.1.call-update) | async-done | bytes 2097168 | tf_op jit(solution)/shard_map/all_gather | solution.py:107
  102.4 4.0 copy.37
  106.4 6.5 %fusion.4 = (f32[128,8]{0,1:T(8,128)S(1)}, f32[8,2048,128]{2,1,0:T(8,128)S(1)}) fusion(f32[8,2048]{1,0:T(8,128)S(1)} %copy.43, f32[128,8]{0,1:T(8,128)S(1)} %copy.42, pred[128,2048]{0,1:T(8,128)(4,1)S(1)} %iota_compare_fusion, bf16[2048,8,64]{0,2,1:T(8,128)(2,1)} %bitcast.83, bf16[128,8,64]{0,2,1:T(8,128)(2,1)S(1)} %bitcast.88), kind=kOutput, calls=%fused_computation.6 | convolution fusion | flops 278920192 | bytes 10952704 | tf_op jit(solution)/shard_map/qhd,khd->qhk/dot_general | solution.py:32
  112.9 3.2 copy-done.2
  116.1 3.1 fusion.2
  119.2 36.6 %all-gather.7.cloned.1.call-done = bf16[2048,1024]{0,1:T(8,128)(2,1)} async-done(((bf16[128,1024]{0,1:T(8,128)(2,1)}), bf16[2048,1024]{0,1:T(8,128)(2,1)}) %all-gather.7.cloned.1.call-update) | async-done | bytes 4194320 | tf_op jit(solution)/shard_map/all_gather | solution.py:109
  155.8 2.5 fusion.46
  158.3 1.8 fusion.48
  160.2 0.8 fusion.10
  161.0 0.8 copy-done.6
  161.8 1.2 multiply_reduce_fusion.1
  162.9 0.1 slice-done.1
  163.1 3.3 multiply_reduce_fusion.2
  166.5 0.5 fusion.49
  167.0 1.0 copy-done.5
  167.9 1.3 fusion.12
  169.3 0.0 all-gather.15.cloned.1.call-start
  169.3 0.5 all-gather.15.cloned.1.call-update
  169.9 0.0 all-gather.13.cloned.1.call-start
  169.9 0.5 all-gather.13.cloned.1.call-update
  170.4 0.2 all-gather.17.cloned.1.call-start
  170.7 0.5 all-gather.17.cloned.1.call-update
  171.2 0.0 reduce-scatter.5.cloned.1.call-start
  171.3 10.9 %reduce-scatter.3.cloned.1.call-done = bf16[64,2048]{1,0:T(8,128)(2,1)} async-done(((bf16[128,2048]{1,0:T(8,128)(2,1)}), bf16[64,2048]{1,0:T(8,128)(2,1)}) %reduce-scatter.3.cloned.1.call-update) | async-done | bytes 262160 | tf_op jit(solution)/shard_map/reduce_scatter | solution.py:119
  182.2 1.1 multiply_reduce_fusion
  183.4 1.1 multiply_convert_fusion
  184.5 8.5 %all_gather.32 = bf16[128,2048]{1,0:T(8,128)(2,1)S(1)} all-gather(bf16[64,2048]{1,0:T(8,128)(2,1)S(1)} %multiply_convert_fusion), channel_id=1, replica_groups=mesh['sp'=16,'tp'=2] {'tp'}, dimensions={0}, use_global_device_ids=true | all-gather | bytes 786432 | tf_op jit(solution)/shard_map/all_gather | solution.py:132
  193.0 65.6 %all-gather.15.cloned.1.call-done = bf16[2048,2048]{1,0:T(8,128)(2,1)} async-done(((bf16[128,2048]{1,0:T(8,128)(2,1)}), bf16[2048,2048]{1,0:T(8,128)(2,1)}) %all-gather.15.cloned.1.call-update) | async-done | bytes 8388624 | tf_op jit(solution)/shard_map/all_gather | solution.py:86
  258.6 4.6 %convolution_convert_fusion.1 = bf16[128,2048]{1,0:T(8,128)(2,1)S(1)} fusion(bf16[128,2048]{1,0:T(8,128)(2,1)S(1)} %all_gather.32, bf16[2048,2048]{1,0:T(8,128)(2,1)} %all-gather.15.cloned.1.call-done), kind=kOutput, calls=%fused_computation.17 | convolution fusion | flops 1074003968 | bytes 9437184 | tf_op jit(solution)/shard_map/dot_general | solution.py:134
  263.2 70.3 %all-gather.13.cloned.1.call-done = bf16[2048,2048]{1,0:T(8,128)(2,1)} async-done(((bf16[128,2048]{1,0:T(8,128)(2,1)}), bf16[2048,2048]{1,0:T(8,128)(2,1)}) %all-gather.13.cloned.1.call-update) | async-done | bytes 8388624 | tf_op jit(solution)/shard_map/all_gather | solution.py:85
  333.5 4.6 %convolution_convert_fusion.2 = bf16[128,2048]{1,0:T(8,128)(2,1)S(1)} fusion(bf16[128,2048]{1,0:T(8,128)(2,1)S(1)} %all_gather.32, bf16[2048,2048]{1,0:T(8,128)(2,1)} %all-gather.13.cloned.1.call-done), kind=kOutput, calls=%fused_computation.18 | convolution fusion | flops 1074003968 | bytes 9437184 | tf_op jit(solution)/shard_map/dot_general | solution.py:133
  338.2 2.2 collective-permute-start
  340.4 0.8 collective-permute-done
  341.2 0.3 maximum_convert_fusion
  341.5 2.0 fusion.15
  343.4 68.5 %all-gather.17.cloned.1.call-done = bf16[2048,2048]{1,0:T(8,128)(2,1)} async-done(((bf16[2048,128]{1,0:T(8,128)(2,1)}), bf16[2048,2048]{1,0:T(8,128)(2,1)}) %all-gather.17.cloned.1.call-update) | async-done | bytes 8388624 | tf_op jit(solution)/shard_map/all_gather | solution.py:87
  412.0 6.3 %convolution_convert_fusion = bf16[128,2048]{1,0:T(8,128)(2,1)} fusion(bf16[2048,2048]{1,0:T(8,128)(2,1)} %all-gather.17.cloned.1.call-done, f32[128,4096]{1,0:T(8,128)} %fusion.15), kind=kOutput, calls=%fused_computation.16 | convolution fusion | flops 1075576832 | bytes 11010048 | tf_op jit(solution)/shard_map/dot_general | solution.py:148
  418.3 13.0 %reduce-scatter.5.cloned.1.call-done = bf16[64,2048]{1,0:T(8,128)(2,1)} async-done(((bf16[128,2048]{1,0:T(8,128)(2,1)}), bf16[64,2048]{1,0:T(8,128)(2,1)}) %reduce-scatter.5.cloned.1.call-update) | async-done | bytes 262160 | tf_op jit(solution)/shard_map/reduce_scatter | solution.py:147
  431.3 1.7 add_convert_fusion
  (48 shorter events, 0.4 us)
Async XLA Ops:
  6.5 159.9 %copy-start = (bf16[512,2048]{1,0:T(8,128)(2,1)S(1)}, bf16[512,2048]{1,0:T(8,128)(2,1)}, u32[]{:S(2)}) copy-start(bf16[512,2048]{1,0:T(8,128)(2,1)} %param.26) | copy-start | bytes 6291460
  6.5 32.8 %copy-start.11 = (f32[128,8]{0,1:T(8,128)S(1)}, f32[128,8]{0,1:T(8,128)}, u32[]{:S(2)}) copy-start(f32[128,8]{0,1:T(8,128)} %param.24) | copy-start | bytes 12292
  6.5 57.7 %all-gather.11.cloned.1.call-start = ((), (), s32[]{:S(2)}) async-start(), calls=%async_computation.4 | async-start | bytes 2228224 | tf_op jit(solution)/shard_map/all_gather | solution.py:113
  7.3 95.1 %all-gather.9.cloned.1.call-start = ((), (), s32[]{:S(2)}) async-start(), calls=%async_computation.3 | async-start | bytes 2228224 | tf_op jit(solution)/shard_map/all_gather | solution.py:107
  8.0 147.8 %all-gather.7.cloned.1.call-start = ((), (), s32[]{:S(2)}) async-start(), calls=%async_computation.2 | async-start | bytes 4456448 | tf_op jit(solution)/shard_map/all_gather | solution.py:109
  10.9 171.4 %reduce-scatter.3.cloned.1.call-start = ((), (), s32[]{:S(2)}) async-start(), calls=%async_computation.5 | async-start | bytes 786432 | tf_op jit(solution)/shard_map/reduce_scatter | solution.py:119
  38.8 25.1 %copy-start.7 = (bf16[128,512]{1,0:T(8,128)(2,1)S(1)}, bf16[128,512]{1,0:T(8,128)(2,1)}, u32[]{:S(2)}) copy-start(bf16[128,512]{1,0:T(8,128)(2,1)} %param.18) | copy-start | bytes 393220
  112.9 3.2 copy-start.2
  119.2 39.1 %copy-start.12 = (bf16[128,512]{1,0:T(8,128)(2,1)S(1)}, bf16[128,512]{1,0:T(8,128)(2,1)}, u32[]{:S(2)}) copy-start(bf16[128,512]{1,0:T(8,128)(2,1)} %param.21) | copy-start | bytes 393220
  158.3 4.6 %slice-start = ((s8[8388608]{0:T(1024)(128)(4,1)}), s8[4194304]{0:T(1024)(128)(4,1)S(1)}, s32[]{:S(2)}) async-start(s8[8388608]{0:T(1024)(128)(4,1)} %bitcast.76), calls=%async_computation.10 | async-start | bytes 8388608
  160.2 1.6 copy-start.6
  160.2 2.9 slice-start.1
  166.3 1.6 copy-start.5
  166.4 4.8 %copy-start.8 = (f32[3,2048]{1,0:T(4,128)S(1)}, f32[3,2048]{1,0:T(4,128)}, u32[]{:S(2)}) copy-start(f32[3,2048]{1,0:T(4,128)} %param.31) | copy-start | bytes 73732
  166.4 4.8 %copy-start.9 = (f32[3,2048]{1,0:T(4,128)S(1)}, f32[3,2048]{1,0:T(4,128)}, u32[]{:S(2)}) copy-start(f32[3,2048]{1,0:T(4,128)} %param.32) | copy-start | bytes 73732
  166.5 15.8 %copy-start.3 = (bf16[64,2048]{1,0:T(8,128)(2,1)S(1)}, bf16[64,2048]{1,0:T(8,128)(2,1)}, u32[]{:S(2)}) copy-start(bf16[64,2048]{1,0:T(8,128)(2,1)} %param.17) | copy-start | bytes 786436
  166.5 16.9 %copy-start.10 = (f32[2048]{0:T(1024)S(1)}, f32[2048]{0:T(1024)}, u32[]{:S(2)}) copy-start(f32[2048]{0:T(1024)} %param.28) | copy-start | bytes 24580
  169.3 89.3 %all-gather.15.cloned.1.call-start = ((), (), s32[]{:S(2)}) async-start(), calls=%async_computation.7 | async-start | bytes 8912896 | tf_op jit(solution)/shard_map/all_gather | solution.py:86
  169.9 163.6 %all-gather.13.cloned.1.call-start = ((), (), s32[]{:S(2)}) async-start(), calls=%async_computation.6 | async-start | bytes 8912896 | tf_op jit(solution)/shard_map/all_gather | solution.py:85
  170.4 241.5 %all-gather.17.cloned.1.call-start = ((), (), s32[]{:S(2)}) async-start(), calls=%async_computation.8 | async-start | bytes 8912896 | tf_op jit(solution)/shard_map/all_gather | solution.py:87
  171.2 260.1 %reduce-scatter.5.cloned.1.call-start = ((), (), s32[]{:S(2)}) async-start(), calls=%async_computation.9 | async-start | bytes 786432 | tf_op jit(solution)/shard_map/reduce_scatter | solution.py:147
  338.2 3.0 collective-permute-start
  343.4 87.8 %copy-start.4 = (bf16[64,2048]{1,0:T(8,128)(2,1)S(1)}, bf16[64,2048]{1,0:T(8,128)(2,1)}, u32[]{:S(2)}) copy-start(bf16[64,2048]{1,0:T(8,128)(2,1)} %reduce-scatter.3.cloned.1.call-done) | copy-start | bytes 786436
  412.0 21.0 %copy-start.1 = (bf16[512,2048]{1,0:T(8,128)(2,1)S(1)}, bf16[512,2048]{1,0:T(8,128)(2,1)}, u32[]{:S(2)}) copy-start(bf16[512,2048]{1,0:T(8,128)(2,1)} %param.26) | copy-start | bytes 6291460
Sparse Core Ops, SparseCore 0:
  9.5 50.1 all-gather.10
  61.8 40.5 all-gather.8
  104.5 51.1 all-gather.6
  169.4 12.7 reduce-scatter.2
  184.2 74.2 all-gather.14
  260.6 72.8 all-gather.12
  335.6 76.2 all-gather.16
  418.4 12.7 reduce-scatter.4
